TPU v7x, 32 devices: a whole 2x2x4 slice. The times are simulated.
32 devices in a mesh: ep: 8 (over z, x), tp: 4 (over y, core).
Axes of the slice: x: 2, y: 2, z: 4, core: 2. Of those that a mesh axis runs over, the one named last changes fastest.
Arguments:
- x_path: bfloat16 [8192, 2048], P('ep', 'tp'), may hold values from -6 to 6
- gate_path: bfloat16 [8192, 2048], P('ep', 'tp'), may hold values from -6 to 6
- conv_taps: float32 [4, 2048], P(None, 'tp'), may hold values from -3 to 3
- decay_gate_w: bfloat16 [2, 16, 128, 128], P(None, 'tp'), may hold values from -0.5 to 0.5
- input_gate_w: bfloat16 [2, 16, 128, 128], P(None, 'tp'), may hold values from -0.5 to 0.5
- decay_rate: float32 [2, 2048], P(None, 'tp'), may hold values from 0 to 1, as said below
- decay_shift: float32 [8192, 16], P('ep', 'tp'), may hold values from -1 to 0, as said below
- expert_in: bfloat16 [512, 2048], P('ep'), may hold values from -6 to 6
- norm_gain: float32 [2048], replicated, may hold values from 0.1 to 1.9
- routes: int32 [512, 2], P('ep'), may hold values from 0 to 7, all different within a row; in each aligned block of 16 rows (0 to 15, 16 to 31, ...) at most 8 rows name the same one
- route_scores: float32 [512, 2], P('ep'), may hold values from 0.1 to 1
- gate_weight: bfloat16 [8, 2048, 4096], P('ep', None, 'tp'), may hold values from -0.125 to 0.125
- up_weight: bfloat16 [8, 2048, 4096], P('ep', None, 'tp'), may hold values from -0.125 to 0.125
- down_weight: bfloat16 [8, 4096, 2048], P('ep', 'tp'), may hold values from -0.09375 to 0.09375
Outputs:
- recurrent_out: bfloat16 [8192, 2048], P('ep', 'tp')
- expert_out: bfloat16 [512, 2048], P(('ep', 'tp'))
Inputs may be any that keep to these rules, and one draw needn't show every extreme that they name: `routes`: in each aligned block of 16 rows no expert is named by more than 8 rows, and in some block some expert is named by exactly 8 rows; each row names 2 different experts. `decay_rate`: positive rates. `decay_shift`: never positive.
All inputs are finite; a program needn't handle non-finite values.
Results may differ from a plain program's by a relative error of at most 0.019.
Values may be sent and summed in bfloat16 or wider, within the bound.
A program may use at most 128 MiB of HBM per device.

v0:
```python
import functools

import jax
import jax.numpy as jnp
from jax import lax
from jax.experimental import pallas as pl
from jax.experimental.pallas import tpu as pltpu
from jax.sharding import PartitionSpec as P

TOP_K = 2
EPSILON = 1e-06
SUB = 8
LANES = 128
EDGE = 16
STEPS = 16
LOG2E = 1.4426950408889634
F32 = jnp.float32
BF16 = jnp.bfloat16
MESH = pl.DeviceIdType.MESH


def remote(src, dst, send, recv, where):
    return pltpu.make_async_remote_copy(
        src_ref=src, dst_ref=dst, send_sem=send, recv_sem=recv, device_id=where, device_id_type=MESH
    )


def kernel(
    n_ep, n_tp, capacity,
    x_ref, gate_hbm, taps_ref, dgw_ref, igw_ref, rate_ref, shift_ref, ein_ref, gain_ref,
    routes_ref, scores_ref, gw_hbm, uw_hbm, dw_hbm,
    rec_hbm, exp_ref,
    xs, yb, af, bf, ab, bb, seg, carry, gathered, halo, gate_v, out_v,
    gw, uw, dw, normed, places, snd, rcv, hid, part, prcv, ret, retrcv, retf,
    local_sem, halo_send, halo_recv, dis_send, dis_recv, sum_send, sum_recv,
    part_send, part_recv, ret_send, ret_recv,
):
    me = lax.axis_index("ep")
    tp = lax.axis_index("tp")
    rows, width = x_ref.shape
    heads = width // LANES
    span = rows // SUB
    tokens, model = ein_ref.shape
    exit_rows = tokens // n_tp
    per_expert = n_tp * capacity
    slots = n_ep * per_expert
    block_slots = n_ep * capacity
    ff = gw_hbm.shape[2]

    loads = [
        pltpu.make_async_copy(gw_hbm.at[0], gw, local_sem.at[0]),
        pltpu.make_async_copy(uw_hbm.at[0], uw, local_sem.at[1]),
        pltpu.make_async_copy(dw_hbm.at[0], dw, local_sem.at[2]),
        pltpu.make_async_copy(gate_hbm, gate_v, local_sem.at[3]),
    ]
    for load in loads:
        load.start()

    barrier = pltpu.get_barrier_semaphore()
    for d in range(1, n_ep):
        pl.semaphore_signal(barrier, inc=1, device_id={"ep": lax.rem(me + d, n_ep)}, device_id_type=MESH)
    for d in range(1, n_tp):
        pl.semaphore_signal(barrier, inc=1, device_id={"tp": lax.rem(tp + d, n_tp)}, device_id_type=MESH)
    pl.semaphore_wait(barrier, n_ep + n_tp - 2)

    up = remote(
        x_ref.at[pl.ds(rows - EDGE, EDGE)], halo.at[0], halo_send.at[0], halo_recv.at[0],
        {"ep": lax.rem(me + 1, n_ep)},
    )
    down = remote(
        x_ref.at[pl.ds(0, EDGE)], halo.at[1], halo_send.at[1], halo_recv.at[1],
        {"ep": lax.rem(me + n_ep - 1, n_ep)},
    )

    @pl.when(me < n_ep - 1)
    def _():
        up.start()

    @pl.when(me > 0)
    def _():
        down.start()

    wide = ein_ref[...].astype(F32)
    scale = lax.rsqrt(jnp.mean(wide * wide, axis=1, keepdims=True) + EPSILON)
    normed[...] = (wide * scale * gain_ref[...]).astype(BF16)
    expert_ids = lax.broadcasted_iota(jnp.int32, (tokens, n_ep), 1)
    first = routes_ref[:, 0:1] == expert_ids
    second = routes_ref[:, 1:2] == expert_ids
    member = (first | second).astype(BF16)
    row_id = lax.broadcasted_iota(jnp.int32, (tokens, tokens), 0)
    col_id = lax.broadcasted_iota(jnp.int32, (tokens, tokens), 1)
    before = (col_id < row_id) & (col_id // exit_rows == row_id // exit_rows)
    ranks = jnp.dot(before.astype(BF16), member, preferred_element_type=F32)
    rank_first = jnp.sum(jnp.where(first, ranks, 0.0), axis=1, keepdims=True).astype(jnp.int32)
    rank_second = jnp.sum(jnp.where(second, ranks, 0.0), axis=1, keepdims=True).astype(jnp.int32)
    places[:, 0:1] = routes_ref[:, 0:1] * capacity + rank_first
    places[:, 1:2] = routes_ref[:, 1:2] * capacity + rank_second
    token_block = lax.broadcasted_iota(jnp.int32, (tokens, 1), 0) // exit_rows
    slot_first = routes_ref[:, 0:1] * per_expert + token_block * capacity + rank_first
    slot_second = routes_ref[:, 1:2] * per_expert + token_block * capacity + rank_second
    slot_ids = lax.broadcasted_iota(jnp.int32, (tokens, slots), 1)
    selector = ((slot_first == slot_ids) | (slot_second == slot_ids)).astype(F32)
    selector = selector.T.astype(BF16)
    for e in range(n_ep):
        snd[e] = jnp.dot(
            selector[e * per_expert : (e + 1) * per_expert], normed[...], preferred_element_type=F32
        ).astype(BF16)
    dispatch = []
    for d in range(1, n_ep):
        peer = lax.rem(me + d, n_ep)
        copy = remote(snd.at[peer], rcv.at[me], dis_send.at[d], dis_recv.at[d], {"ep": peer})
        copy.start()
        dispatch.append(copy)
    rcv_own = pltpu.make_async_copy(snd.at[me], rcv.at[me], local_sem.at[4])
    rcv_own.start()

    def widen(i, c):
        r = pl.multiple_of(i * LANES, LANES)
        for h in range(heads):
            xs[h, pl.ds(SUB + r, LANES), :] = x_ref[
                pl.ds(r, LANES), h * LANES : (h + 1) * LANES
            ].astype(F32)
        return c

    lax.fori_loop(0, rows // LANES, widen, 0)

    @pl.when(me == 0)
    def _():
        halo[0] = jnp.zeros((EDGE, width), BF16)

    @pl.when(me == n_ep - 1)
    def _():
        halo[1] = jnp.zeros((EDGE, width), BF16)

    @pl.when(me > 0)
    def _():
        up.wait_recv()

    @pl.when(me < n_ep - 1)
    def _():
        down.wait_recv()

    lower = halo[0].astype(F32)
    upper = halo[1].astype(F32)
    for h in range(heads):
        lanes = slice(h * LANES, (h + 1) * LANES)
        xs[h, 0:SUB, :] = lower[EDGE - SUB : EDGE, lanes]
        xs[h, SUB + rows : 2 * SUB + rows, :] = upper[0:SUB, lanes]

    ones = jnp.ones((SUB, LANES), F32)
    zeros = jnp.zeros((SUB, LANES), F32)
    for h in range(heads):
        lanes = slice(h * LANES, (h + 1) * LANES)
        taps = [taps_ref[k : k + 1, lanes] for k in range(4)]
        weights = jnp.concatenate(
            [dgw_ref[0, h], dgw_ref[1, h], igw_ref[0, h], igw_ref[1, h]], axis=1
        )
        rates = [rate_ref[d : d + 1, lanes] * (-8.0) for d in range(2)]

        def chunk(c, state, h=h, taps=taps, weights=weights, rates=rates):
            total_f, end_f, total_b, end_b = state
            s0 = c * STEPS
            window = [
                xs[h, pl.ds(SUB - 2 + s0 + i, SUB, stride=span), :] for i in range(STEPS + 3)
            ]
            conv = []
            for i in range(STEPS):
                total = window[i] * taps[0]
                for k in range(1, 4):
                    total = total + window[i + k] * taps[k]
                conv.append(total)
            conv = jnp.concatenate(conv, axis=0).astype(BF16)
            pre = jnp.dot(conv, weights, preferred_element_type=F32)
            conv = conv.astype(F32)
            shift = jnp.concatenate(
                [
                    jnp.broadcast_to(
                        shift_ref[pl.ds(s0 + i, SUB, stride=span), :][:, h : h + 1], (SUB, LANES)
                    )
                    for i in range(STEPS)
                ],
                axis=0,
            )
            place = pl.ds(pl.multiple_of(s0 * SUB, STEPS * SUB), STEPS * SUB)
            pairs = []
            for d, (a_ref, b_ref) in enumerate(((af, bf), (ab, bb))):
                gate = 1.0 / (1.0 + jnp.exp(-pre[:, d * LANES : (d + 1) * LANES]))
                log_decay = gate * rates[d] + shift
                decay = jnp.exp(log_decay)
                x2 = 2.0 * log_decay
                series = -x2 * (1.0 + x2 * (0.5 + x2 * (1.0 / 6.0 + x2 * (1.0 / 24.0))))
                square = jnp.where(x2 > -0.1, series, 1.0 - decay * decay)
                root = jnp.where(square > 0.0, square * lax.rsqrt(square), 0.0)
                half = 0.5 * pre[:, (2 + d) * LANES : (3 + d) * LANES]
                drive = root * (0.5 + 0.5 * jnp.tanh(half)) * conv
                a_ref[h, place, :] = decay
                b_ref[h, place, :] = drive
                pairs.append((decay, drive))
            for i in range(STEPS):
                part_rows = slice(i * SUB, (i + 1) * SUB)
                a, b = pairs[0][0][part_rows], pairs[0][1][part_rows]
                end_f = a * end_f + b
                total_f = total_f * a
                a, b = pairs[1][0][part_rows], pairs[1][1][part_rows]
                end_b = end_b + total_b * b
                total_b = total_b * a
            return total_f, end_f, total_b, end_b

        state = lax.fori_loop(0, span // STEPS, chunk, (ones, zeros, ones, zeros))
        for i in range(4):
            seg[i, :, lanes] = state[i]

    one_row = jnp.ones((1, width), F32)
    zero_row = jnp.zeros((1, width), F32)
    total_f, end_f, total_b, end_b = one_row, zero_row, one_row, zero_row
    for k in range(SUB):
        end_f = seg[0, k : k + 1, :] * end_f + seg[1, k : k + 1, :]
        total_f = total_f * seg[0, k : k + 1, :]
        end_b = end_b + total_b * seg[3, k : k + 1, :]
        total_b = total_b * seg[2, k : k + 1, :]
    gathered[me, 0:1, :] = total_f
    gathered[me, 1:2, :] = end_f
    gathered[me, 2:3, :] = total_b
    gathered[me, 3:4, :] = end_b
    gathered[me, 4:8, :] = jnp.zeros((4, width), F32)
    sums = []
    for d in range(1, n_ep):
        peer = lax.rem(me + d, n_ep)
        copy = remote(gathered.at[me], gathered.at[me], sum_send.at[d], sum_recv.at[d], {"ep": peer})
        copy.start()
        sums.append(copy)

    rcv_own.wait()
    for copy in dispatch:
        copy.wait()
    for load in loads[:3]:
        load.wait()
    arrived = rcv.reshape(slots, model)
    tile = min(256, ff)

    def project(n, c):
        cols = pl.ds(pl.multiple_of(n * tile, tile), tile)
        gate_pre = jnp.dot(arrived[...], gw[:, cols], preferred_element_type=F32)
        up_pre = jnp.dot(arrived[...], uw[:, cols], preferred_element_type=F32)
        hid[:, cols] = (gate_pre / (1.0 + jnp.exp(-gate_pre)) * up_pre).astype(BF16)
        return c

    lax.fori_loop(0, ff // tile, project, 0)
    partials = []
    for d in list(range(1, n_tp)) + [0]:
        peer = lax.rem(tp + d, n_tp)
        out_row = lax.broadcasted_iota(jnp.int32, (block_slots, slots), 0)
        in_row = lax.broadcasted_iota(jnp.int32, (block_slots, slots), 1)
        source = (out_row // capacity) * per_expert + peer * capacity + out_row % capacity
        pick = (source == in_row).astype(BF16)
        picked = jnp.dot(pick, hid[...], preferred_element_type=F32).astype(BF16)
        value = jnp.dot(picked, dw[...], preferred_element_type=F32).astype(BF16)
        if d == 0:
            prcv[0] = value
        else:
            part[d] = value
            copy = remote(part.at[d], prcv.at[d], part_send.at[d], part_recv.at[d], {"tp": peer})
            copy.start()
            partials.append(copy)

    for copy in sums:
        copy.wait()
    carry_f, carry_b = zero_row, zero_row
    for j in range(n_ep):
        carry_f = jnp.where(j < me, gathered[j, 0:1, :] * carry_f + gathered[j, 1:2, :], carry_f)
    for j in range(n_ep - 1, -1, -1):
        carry_b = jnp.where(j > me, gathered[j, 2:3, :] * carry_b + gathered[j, 3:4, :], carry_b)
    for k in range(SUB):
        carry[0, k : k + 1, :] = carry_f
        carry_f = seg[0, k : k + 1, :] * carry_f + seg[1, k : k + 1, :]
    for k in range(SUB - 1, -1, -1):
        carry[1, k : k + 1, :] = carry_b
        carry_b = seg[2, k : k + 1, :] * carry_b + seg[3, k : k + 1, :]

    def advance(c, state):
        state = list(state)
        for i in range(SUB):
            s = c * SUB + i
            r = span - 1 - s
            here = pl.ds(pl.multiple_of(s * SUB, SUB), SUB)
            there = pl.ds(pl.multiple_of(r * SUB, SUB), SUB)
            for h in range(heads):
                state[h] = af[h, here, :] * state[h] + bf[h, here, :]
                xs[h, pl.ds(s, SUB, stride=span), :] = state[h]
                g = heads + h
                state[g] = ab[h, there, :] * state[g] + bb[h, there, :]
                yb[h, pl.ds(r, SUB, stride=span), :] = state[g]
        return tuple(state)

    start = [carry[d, :, h * LANES : (h + 1) * LANES] for d in range(2) for h in range(heads)]
    lax.fori_loop(0, span // SUB, advance, tuple(start))
    loads[3].wait()
    block = 64

    def finish(i, c):
        here = pl.ds(pl.multiple_of(i * block, block), block)
        for h in range(heads):
            lanes = slice(h * LANES, (h + 1) * LANES)
            g = gate_v[here, lanes].astype(F32)
            inner = 0.7978845608028654 * (g + 0.044715 * (g * g * g))
            gated = g * (0.5 * (1.0 + jnp.tanh(inner)))
            out_v[here, lanes] = ((xs[h, here, :] + yb[h, here, :]) * gated).astype(BF16)
        return c

    lax.fori_loop(0, rows // block, finish, 0)
    store = pltpu.make_async_copy(out_v, rec_hbm, local_sem.at[5])
    store.start()

    for copy in partials:
        copy.wait()
    summed = prcv[0].astype(F32)
    for d in range(1, n_tp):
        summed = summed + prcv[d].astype(F32)
    for e in range(n_ep):
        ret[e] = summed[e * capacity : (e + 1) * capacity].astype(BF16)
    backs = []
    for d in range(1, n_ep):
        peer = lax.rem(me + d, n_ep)
        copy = remote(ret.at[peer], retrcv.at[me], ret_send.at[d], ret_recv.at[d], {"ep": peer})
        copy.start()
        backs.append(copy)
    retrcv[me] = ret[me]
    for copy in backs:
        copy.wait()
    for e in range(n_ep):
        retf[e * capacity : (e + 1) * capacity, :] = retrcv[e].astype(F32)
    returned = retf[...].astype(BF16)
    own = pl.ds(pl.multiple_of(tp * exit_rows, exit_rows), exit_rows)
    scores = scores_ref[own, :]
    shares = scores / jnp.sum(scores, axis=1, keepdims=True)
    ids = lax.broadcasted_iota(jnp.int32, (exit_rows, block_slots), 1)
    total = jnp.zeros((exit_rows, model), F32)
    for k in range(TOP_K):
        pick = (places[own, k : k + 1] == ids).astype(BF16)
        total = total + shares[:, k : k + 1] * jnp.dot(pick, returned, preferred_element_type=F32)
    exp_ref[...] = total.astype(BF16)

    @pl.when(me < n_ep - 1)
    def _():
        up.wait_send()

    @pl.when(me > 0)
    def _():
        down.wait_send()

    store.wait()


def local(
    x_path, gate_path, conv_taps, decay_gate_w, input_gate_w, decay_rate, decay_shift, expert_in,
    norm_gain, routes, route_scores, gate_weight, up_weight, down_weight,
):
    n_ep, n_tp = lax.axis_size("ep"), lax.axis_size("tp")
    rows, width = x_path.shape
    heads = width // LANES
    tokens, model = expert_in.shape
    ff = gate_weight.shape[2]
    exit_rows = tokens // n_tp
    capacity = max(2, 2 * exit_rows * TOP_K // n_ep)
    per_expert = n_tp * capacity
    block_slots = n_ep * capacity
    vmem = pl.BlockSpec(memory_space=pltpu.VMEM)
    hbm = pl.BlockSpec(memory_space=pl.ANY)
    pair = pltpu.VMEM((heads, rows, LANES), F32)
    dma = pltpu.SemaphoreType.DMA
    return pl.pallas_call(
        functools.partial(kernel, n_ep, n_tp, capacity),
        out_shape=(
            jax.ShapeDtypeStruct((rows, width), BF16),
            jax.ShapeDtypeStruct((exit_rows, model), BF16),
        ),
        in_specs=[vmem, hbm] + [vmem] * 9 + [hbm] * 3,
        out_specs=(hbm, vmem),
        scratch_shapes=[
            pltpu.VMEM((heads, rows + 2 * SUB, LANES), F32),
            pair, pair, pair, pair, pair,
            pltpu.VMEM((4, SUB, width), F32),
            pltpu.VMEM((2, SUB, width), F32),
            pltpu.VMEM((n_ep, SUB, width), F32),
            pltpu.VMEM((2, EDGE, width), BF16),
            pltpu.VMEM((rows, width), BF16),
            pltpu.VMEM((rows, width), BF16),
            pltpu.VMEM((model, ff), BF16),
            pltpu.VMEM((model, ff), BF16),
            pltpu.VMEM((ff, model), BF16),
            pltpu.VMEM((tokens, model), BF16),
            pltpu.VMEM((tokens, TOP_K), jnp.int32),
            pltpu.VMEM((n_ep, per_expert, model), BF16),
            pltpu.VMEM((n_ep, per_expert, model), BF16),
            pltpu.VMEM((n_ep * per_expert, ff), BF16),
            pltpu.VMEM((n_tp, block_slots, model), BF16),
            pltpu.VMEM((n_tp, block_slots, model), BF16),
            pltpu.VMEM((n_ep, capacity, model), BF16),
            pltpu.VMEM((n_ep, capacity, model), BF16),
            pltpu.VMEM((block_slots, model), F32),
            dma((6,)), dma((2,)), dma((2,)), dma((n_ep,)), dma((n_ep,)), dma((n_ep,)), dma((n_ep,)),
            dma((n_tp,)), dma((n_tp,)), dma((n_ep,)), dma((n_ep,)),
        ],
        compiler_params=pltpu.CompilerParams(
            collective_id=0, has_side_effects=True, vmem_limit_bytes=62 * 1024 * 1024
        ),
        name="layer",
    )(
        x_path, gate_path, conv_taps, decay_gate_w, input_gate_w, decay_rate, decay_shift,
        expert_in, norm_gain.reshape(1, model), routes, route_scores,
        gate_weight, up_weight, down_weight,
    )


def solution(mesh):
    in_specs = (
        P("ep", "tp"),
        P("ep", "tp"),
        P(None, "tp"),
        P(None, "tp", None, None),
        P(None, "tp", None, None),
        P(None, "tp"),
        P("ep", "tp"),
        P("ep", None),
        P(),
        P("ep", None),
        P("ep", None),
        P("ep", None, "tp"),
        P("ep", None, "tp"),
        P("ep", "tp", None),
    )
    out_specs = (P("ep", "tp"), P(("ep", "tp"), None))
    return jax.shard_map(local, mesh=mesh, in_specs=in_specs, out_specs=out_specs, check_vma=False)
```

profile of v0, /device:TPU:1, one launch (start us, length us, event | category | flops | bytes accessed | tf_op | source)
XLA Modules:
  0.0 64.8 jit_solution(6246357411444041124)
XLA Ops:
  0.6 1.4 %copy.17.routes_ref = s32[64,2]{1,0:T(8,128)} copy(s32[64,2]{0,1:T(2,128)} %param.23) | data formatting | bytes 1024 | tf_op args[9]
  2.0 1.4 %copy.18.scores_ref = f32[64,2]{1,0:T(8,128)} copy(f32[64,2]{0,1:T(2,128)} %param.24) | data formatting | bytes 1024 | tf_op args[10]
  3.4 1.7 %copy.16.shift_ref = f32[1024,4]{1,0:T(8,128)} copy(f32[1024,4]{0,1:T(4,128)} %param.20) | data formatting | bytes 32768 | tf_op args[6]
  5.1 55.9 %layer.1 = (bf16[1024,512]{1,0:T(8,128)(2,1)}, bf16[16,2048]{1,0:T(8,128)(2,1)}) custom-call(bf16[1024,512]{1,0:T(8,128)(2,1)} %x_ref.1, bf16[1024,512]{1,0:T(8,128)(2,1)} %gate_hbm.1, f32[4,512]{1,0:T(4,128)} %taps_ref.1, bf16[2,4,128,128]{3,2,1,0:T(8,128)(2,1)} %dgw_ref.1, bf16[2,4,128,128]{3,2,1,0:T(8,128)(2,1)} %igw_ref.1, f32[2,512]{1,0:T(2,128)} %rate_ref.1, ...), custom_call_target="tpu_custom_call" | custom-call | tf_op jit(solution)/shard_map/layer/pallas_call | solution.py:371
  61.0 2.3 %copy.21 = bf16[1024,512]{1,0:T(8,128)(2,1)} copy(bf16[1024,512]{1,0:T(8,128)(2,1)} %get-tuple-element.4) | data formatting | bytes 2097152
  63.3 1.5 %copy.22 = bf16[16,2048]{1,0:T(8,128)(2,1)} copy(bf16[16,2048]{1,0:T(8,128)(2,1)} %get-tuple-element.5) | data formatting | bytes 131072
where the time goes:
time: 65.1 us; the launch traced here: 64.8 us
  Pallas kernels  55.9 us (86%)
  local copies, waits for them, and re-layouts  8.23 us (13%)
    pallas_call x1, Pallas kernels, local(): pl.pallas_call(functools.partial(kernel, n_ep, n_tp, capacity), out_shape...  55.9 us
    unnamed x5, local copies, waits for them, and re-layouts  8.23 us

commit v1 on v0

--- a/solution.py
+++ b/solution.py
@@ -17,6 +17,9 @@
 F32 = jnp.float32
 BF16 = jnp.bfloat16
 MESH = pl.DeviceIdType.MESH
+PIECES = 2
+SHARE_AT = (2, 3)
+RELAY_AT = (4, 4)
 
 
 def remote(src, dst, send, recv, where):
@@ -31,9 +34,10 @@
     routes_ref, scores_ref, gw_hbm, uw_hbm, dw_hbm,
     rec_hbm, exp_ref,
     xs, yb, af, bf, ab, bb, seg, carry, gathered, halo, gate_v, out_v,
-    gw, uw, dw, normed, places, snd, rcv, hid, part, prcv, ret, retrcv, retf,
-    local_sem, halo_send, halo_recv, dis_send, dis_recv, sum_send, sum_recv,
-    part_send, part_recv, ret_send, ret_recv,
+    gw, uw, dw, normed, meta, shift_seg, snd, got, stage, rcv, hid, part, pairs_in, mixed, across,
+    ret, retrcv,
+    local_sem, halo_send, halo_recv, dis_send, dis_recv, row_send, row_recv, fwd_send, fwd_recv,
+    pair_send, pair_recv, far_send, far_recv, sum_send, sum_recv, ret_send, ret_recv,
 ):
     me = lax.axis_index("ep")
     tp = lax.axis_index("tp")
@@ -42,10 +46,14 @@
     span = rows // SUB
     tokens, model = ein_ref.shape
     exit_rows = tokens // n_tp
-    per_expert = n_tp * capacity
-    slots = n_ep * per_expert
     block_slots = n_ep * capacity
+    core, n_y = lax.rem(tp, 2), n_tp // 2
+    y = tp // 2
+    partner = y * 2 + 1 - core
+    far_ys = [lax.rem(y + d, n_y) for d in range(1, n_y)]
     ff = gw_hbm.shape[2]
+    wide_piece = model // PIECES
+    pieces = [slice(q * wide_piece, (q + 1) * wide_piece) for q in range(PIECES)]
 
     loads = [
         pltpu.make_async_copy(gw_hbm.at[0], gw, local_sem.at[0]),
@@ -83,36 +91,73 @@
     wide = ein_ref[...].astype(F32)
     scale = lax.rsqrt(jnp.mean(wide * wide, axis=1, keepdims=True) + EPSILON)
     normed[...] = (wide * scale * gain_ref[...]).astype(BF16)
-    expert_ids = lax.broadcasted_iota(jnp.int32, (tokens, n_ep), 1)
-    first = routes_ref[:, 0:1] == expert_ids
-    second = routes_ref[:, 1:2] == expert_ids
+    first_route, second_route = routes_ref[0:1, :], routes_ref[1:2, :]
+    expert_ids = lax.broadcasted_iota(jnp.int32, (n_ep, tokens), 0)
+    first = first_route == expert_ids
+    second = second_route == expert_ids
     member = (first | second).astype(BF16)
     row_id = lax.broadcasted_iota(jnp.int32, (tokens, tokens), 0)
     col_id = lax.broadcasted_iota(jnp.int32, (tokens, tokens), 1)
-    before = (col_id < row_id) & (col_id // exit_rows == row_id // exit_rows)
-    ranks = jnp.dot(before.astype(BF16), member, preferred_element_type=F32)
-    rank_first = jnp.sum(jnp.where(first, ranks, 0.0), axis=1, keepdims=True).astype(jnp.int32)
-    rank_second = jnp.sum(jnp.where(second, ranks, 0.0), axis=1, keepdims=True).astype(jnp.int32)
-    places[:, 0:1] = routes_ref[:, 0:1] * capacity + rank_first
-    places[:, 1:2] = routes_ref[:, 1:2] * capacity + rank_second
-    token_block = lax.broadcasted_iota(jnp.int32, (tokens, 1), 0) // exit_rows
-    slot_first = routes_ref[:, 0:1] * per_expert + token_block * capacity + rank_first
-    slot_second = routes_ref[:, 1:2] * per_expert + token_block * capacity + rank_second
-    slot_ids = lax.broadcasted_iota(jnp.int32, (tokens, slots), 1)
-    selector = ((slot_first == slot_ids) | (slot_second == slot_ids)).astype(F32)
-    selector = selector.T.astype(BF16)
+    before = (row_id < col_id) & (row_id // exit_rows == col_id // exit_rows)
+    ranks = jnp.dot(member, before.astype(BF16), preferred_element_type=F32)
+    rank_first = jnp.sum(jnp.where(first, ranks, 0.0), axis=0, keepdims=True).astype(jnp.int32)
+    rank_second = jnp.sum(jnp.where(second, ranks, 0.0), axis=0, keepdims=True).astype(jnp.int32)
+    slot_first = first_route * capacity + rank_first
+    slot_second = second_route * capacity + rank_second
+    scores = scores_ref[...]
+    shares = scores / (scores[0:1] + scores[1:2])
+    meta[...] = jnp.concatenate(
+        [slot_first.astype(F32), slot_second.astype(F32), shares, jnp.zeros((4, tokens), F32)], axis=0
+    ).T
+    is_own = lax.broadcasted_iota(jnp.int32, (1, tokens), 1) // exit_rows == tp
+    slot_ids = lax.broadcasted_iota(jnp.int32, (block_slots, tokens), 0)
+    selector = ((slot_first == slot_ids) | (slot_second == slot_ids)) & is_own
+    stage[...] = jnp.dot(selector.astype(BF16), normed[...], preferred_element_type=F32)
     for e in range(n_ep):
-        snd[e] = jnp.dot(
-            selector[e * per_expert : (e + 1) * per_expert], normed[...], preferred_element_type=F32
-        ).astype(BF16)
+        snd[e] = stage[e * capacity : (e + 1) * capacity, :].astype(BF16)
+    peer_order = list(range(1, n_ep))
     dispatch = []
-    for d in range(1, n_ep):
-        peer = lax.rem(me + d, n_ep)
-        copy = remote(snd.at[peer], rcv.at[me], dis_send.at[d], dis_recv.at[d], {"ep": peer})
-        copy.start()
-        dispatch.append(copy)
-    rcv_own = pltpu.make_async_copy(snd.at[me], rcv.at[me], local_sem.at[4])
-    rcv_own.start()
+    for q, cols in enumerate(pieces):
+        copies = []
+        for d in peer_order:
+            peer = lax.rem(me + d, n_ep)
+            copy = remote(
+                snd.at[peer, :, cols], got.at[me, :, cols], dis_send.at[d, q], dis_recv.at[d, q],
+                {"ep": peer},
+            )
+            copy.start()
+            copies.append(copy)
+        dispatch.append(copies)
+    got[me] = snd[me]
+    rows_sent, forwarded = {}, []
+
+    def share_rows(q):
+        cols = pieces[q]
+        for copy in dispatch[q]:
+            copy.wait()
+        for e in range(n_ep):
+            stage[e * capacity : (e + 1) * capacity, cols] = got[e, :, cols].astype(F32)
+        rcv[tp, :, cols] = stage[:, cols].astype(BF16)
+        own_rows = rcv.at[tp, :, cols]
+        rows_sent[q] = []
+        for d in range(n_y):
+            there = far_ys[d] * 2 + core if d < n_y - 1 else partner
+            copy = remote(own_rows, own_rows, row_send.at[d, q], row_recv.at[d, q], {"tp": there})
+            copy.start()
+            rows_sent[q].append(copy)
+
+    def forward_rows(q):
+        forwarded.append(rows_sent[q][-1])
+        for d in range(1, n_y):
+            rows_sent[q][d - 1].wait()
+            rows_far = rcv.at[lax.rem(y - d + n_y, n_y) * 2 + core, :, pieces[q]]
+            copy = remote(rows_far, rows_far, fwd_send.at[d, q], fwd_recv.at[d, q], {"tp": partner})
+            copy.start()
+            forwarded.append(copy)
+
+    for h in range(heads):
+        for k in range(SUB):
+            shift_seg[h, k : k + 1, :] = shift_ref[h : h + 1, k * span : (k + 1) * span]
 
     def widen(i, c):
         r = pl.multiple_of(i * LANES, LANES)
@@ -147,9 +192,17 @@
         xs[h, 0:SUB, :] = lower[EDGE - SUB : EDGE, lanes]
         xs[h, SUB + rows : 2 * SUB + rows, :] = upper[0:SUB, lanes]
 
+    relays = []
+    for q in range(PIECES):
+        relays.append((SHARE_AT[q] * heads // 4, share_rows, q))
+        relays.append((RELAY_AT[q] * heads // 4, forward_rows, q))
+    relays.sort(key=lambda relay: relay[0])
     ones = jnp.ones((SUB, LANES), F32)
     zeros = jnp.zeros((SUB, LANES), F32)
     for h in range(heads):
+        for at, act, q in relays:
+            if h == at:
+                act(q)
         lanes = slice(h * LANES, (h + 1) * LANES)
         taps = [taps_ref[k : k + 1, lanes] for k in range(4)]
         weights = jnp.concatenate(
@@ -172,10 +225,11 @@
             conv = jnp.concatenate(conv, axis=0).astype(BF16)
             pre = jnp.dot(conv, weights, preferred_element_type=F32)
             conv = conv.astype(F32)
+            rolled = pltpu.roll(shift_seg[h], lax.rem(span - s0, span), 1)
             shift = jnp.concatenate(
                 [
                     jnp.broadcast_to(
-                        shift_ref[pl.ds(s0 + i, SUB, stride=span), :][:, h : h + 1], (SUB, LANES)
+                        rolled[:, i : i + 1], (SUB, LANES)
                     )
                     for i in range(STEPS)
                 ],
@@ -230,12 +284,14 @@
         copy.start()
         sums.append(copy)
 
-    rcv_own.wait()
-    for copy in dispatch:
+    for at, act, q in relays:
+        if at >= heads:
+            act(q)
+    for copy in forwarded:
         copy.wait()
     for load in loads[:3]:
         load.wait()
-    arrived = rcv.reshape(slots, model)
+    arrived = rcv.reshape(n_tp * block_slots, model)
     tile = min(256, ff)
 
     def project(n, c):
@@ -246,22 +302,33 @@
         return c
 
     lax.fori_loop(0, ff // tile, project, 0)
-    partials = []
-    for d in list(range(1, n_tp)) + [0]:
-        peer = lax.rem(tp + d, n_tp)
-        out_row = lax.broadcasted_iota(jnp.int32, (block_slots, slots), 0)
-        in_row = lax.broadcasted_iota(jnp.int32, (block_slots, slots), 1)
-        source = (out_row // capacity) * per_expert + peer * capacity + out_row % capacity
-        pick = (source == in_row).astype(BF16)
-        picked = jnp.dot(pick, hid[...], preferred_element_type=F32).astype(BF16)
-        value = jnp.dot(picked, dw[...], preferred_element_type=F32).astype(BF16)
-        if d == 0:
-            prcv[0] = value
-        else:
-            part[d] = value
-            copy = remote(part.at[d], prcv.at[d], part_send.at[d], part_recv.at[d], {"tp": peer})
+
+    def reduce_part(block, cols):
+        here = pl.ds(pl.multiple_of(block * block_slots, block_slots), block_slots)
+        return jnp.dot(hid[here, :], dw[:, cols], preferred_element_type=F32).astype(BF16)
+
+    pair_copies, far_copies = {}, {}
+    for q, cols in enumerate(pieces):
+        for d in list(range(1, n_y)) + [0]:
+            part[d, :, cols] = reduce_part(lax.rem(y + d, n_y) * 2 + 1 - core, cols)
+            copy = remote(
+                part.at[d, :, cols], pairs_in.at[d, :, cols], pair_send.at[d, q], pair_recv.at[d, q],
+                {"tp": partner},
+            )
             copy.start()
-            partials.append(copy)
+            pair_copies[d, q] = copy
+        for d in range(1, n_y):
+            far = lax.rem(y + d, n_y)
+            value = reduce_part(far * 2 + core, cols)
+            pair_copies[d, q].wait()
+            mixed[d, :, cols] = (value.astype(F32) + pairs_in[d, :, cols].astype(F32)).astype(BF16)
+            copy = remote(
+                mixed.at[d, :, cols], across.at[d, :, cols], far_send.at[d, q], far_recv.at[d, q],
+                {"tp": far * 2 + core},
+            )
+            copy.start()
+            far_copies[d, q] = copy
+        across[0, :, cols] = reduce_part(tp, cols)
 
     for copy in sums:
         copy.wait()
@@ -294,6 +361,27 @@
 
     start = [carry[d, :, h * LANES : (h + 1) * LANES] for d in range(2) for h in range(heads)]
     lax.fori_loop(0, span // SUB, advance, tuple(start))
+    backs = []
+    for q, cols in enumerate(pieces):
+        pair_copies[0, q].wait()
+        summed = across[0, :, cols].astype(F32) + pairs_in[0, :, cols].astype(F32)
+        for d in range(1, n_y):
+            far_copies[d, q].wait()
+            summed = summed + across[d, :, cols].astype(F32)
+        stage[:, cols] = summed
+        for e in range(n_ep):
+            ret[e, :, cols] = stage[e * capacity : (e + 1) * capacity, cols].astype(BF16)
+        copies = []
+        for d in peer_order:
+            peer = lax.rem(me + d, n_ep)
+            copy = remote(
+                ret.at[peer, :, cols], retrcv.at[me, :, cols], ret_send.at[d, q], ret_recv.at[d, q],
+                {"ep": peer},
+            )
+            copy.start()
+            copies.append(copy)
+        backs.append(copies)
+    retrcv[me] = ret[me]
     loads[3].wait()
     block = 64
 
@@ -311,44 +399,63 @@
     store = pltpu.make_async_copy(out_v, rec_hbm, local_sem.at[5])
     store.start()
 
-    for copy in partials:
+    own = pl.ds(pl.multiple_of(tp * exit_rows, exit_rows), exit_rows)
+    own_meta = meta[own, :]
+    ids = lax.broadcasted_iota(jnp.int32, (exit_rows, block_slots), 1)
+    picks = [(own_meta[:, k : k + 1].astype(jnp.int32) == ids).astype(BF16) for k in range(TOP_K)]
+    for q, cols in enumerate(pieces):
+        for copy in backs[q]:
+            copy.wait()
+        for e in range(n_ep):
+            stage[e * capacity : (e + 1) * capacity, cols] = retrcv[e, :, cols].astype(F32)
+        returned = stage[:, cols].astype(BF16)
+        total = jnp.zeros((exit_rows, wide_piece), F32)
+        for k in range(TOP_K):
+            chosen = jnp.dot(picks[k], returned, preferred_element_type=F32)
+            total = total + own_meta[:, TOP_K + k : TOP_K + k + 1] * chosen
+        exp_ref[:, cols] = total.astype(BF16)
+
+    @pl.when(me < n_ep - 1)
+    def _():
+        up.wait_send()
+
+    @pl.when(me > 0)
+    def _():
+        down.wait_send()
+
+    store.wait()
+
+
+def hand_over_kernel(rec_ref, exp_ref, rec_out, exp_out, rec_v, exp_v, in_sem, out_sem):
+    rows = rec_ref.shape[0]
+    step = rows // PIECES
+    routes = [
+        (rec_ref.at[pl.ds(i * step, step)], rec_v.at[pl.ds(i * step, step)], rec_out.at[pl.ds(i * step, step)])
+        for i in range(PIECES)
+    ] + [(exp_ref, exp_v, exp_out)]
+    ins = [pltpu.make_async_copy(a, b, in_sem.at[i]) for i, (a, b, _) in enumerate(routes)]
+    outs = [pltpu.make_async_copy(b, c, out_sem.at[i]) for i, (_, b, c) in enumerate(routes)]
+    for copy in ins:
+        copy.start()
+    for copy, then in zip(ins, outs):
         copy.wait()
-    summed = prcv[0].astype(F32)
-    for d in range(1, n_tp):
-        summed = summed + prcv[d].astype(F32)
-    for e in range(n_ep):
-        ret[e] = summed[e * capacity : (e + 1) * capacity].astype(BF16)
-    backs = []
-    for d in range(1, n_ep):
-        peer = lax.rem(me + d, n_ep)
-        copy = remote(ret.at[peer], retrcv.at[me], ret_send.at[d], ret_recv.at[d], {"ep": peer})
-        copy.start()
-        backs.append(copy)
-    retrcv[me] = ret[me]
-    for copy in backs:
+        then.start()
+    for copy in outs:
         copy.wait()
-    for e in range(n_ep):
-        retf[e * capacity : (e + 1) * capacity, :] = retrcv[e].astype(F32)
-    returned = retf[...].astype(BF16)
-    own = pl.ds(pl.multiple_of(tp * exit_rows, exit_rows), exit_rows)
-    scores = scores_ref[own, :]
-    shares = scores / jnp.sum(scores, axis=1, keepdims=True)
-    ids = lax.broadcasted_iota(jnp.int32, (exit_rows, block_slots), 1)
-    total = jnp.zeros((exit_rows, model), F32)
-    for k in range(TOP_K):
-        pick = (places[own, k : k + 1] == ids).astype(BF16)
-        total = total + shares[:, k : k + 1] * jnp.dot(pick, returned, preferred_element_type=F32)
-    exp_ref[...] = total.astype(BF16)
-
-    @pl.when(me < n_ep - 1)
-    def _():
-        up.wait_send()
-
-    @pl.when(me > 0)
-    def _():
-        down.wait_send()
-
-    store.wait()
+
+
+def hand_over(recurrent, expert):
+    hbm = pl.BlockSpec(memory_space=pl.ANY)
+    shapes = [jax.ShapeDtypeStruct(a.shape, a.dtype) for a in (recurrent, expert)]
+    return pl.pallas_call(
+        hand_over_kernel,
+        out_shape=tuple(shapes),
+        in_specs=[hbm, hbm],
+        out_specs=(hbm, hbm),
+        scratch_shapes=[pltpu.VMEM(a.shape, a.dtype) for a in shapes]
+        + [pltpu.SemaphoreType.DMA((PIECES + 1,))] * 2,
+        name="hand_over",
+    )(recurrent, expert)
 
 
 def local(
@@ -362,13 +469,16 @@
     ff = gate_weight.shape[2]
     exit_rows = tokens // n_tp
     capacity = max(2, 2 * exit_rows * TOP_K // n_ep)
-    per_expert = n_tp * capacity
     block_slots = n_ep * capacity
+    n_y = n_tp // 2
+    rows_of_tp = pltpu.VMEM((n_tp, block_slots, model), BF16)
+    rows_of_y = pltpu.VMEM((n_y, block_slots, model), BF16)
     vmem = pl.BlockSpec(memory_space=pltpu.VMEM)
     hbm = pl.BlockSpec(memory_space=pl.ANY)
     pair = pltpu.VMEM((heads, rows, LANES), F32)
     dma = pltpu.SemaphoreType.DMA
-    return pl.pallas_call(
+    over_ep, over_y = dma((n_ep, PIECES)), dma((n_y, PIECES))
+    recurrent, expert = pl.pallas_call(
         functools.partial(kernel, n_ep, n_tp, capacity),
         out_shape=(
             jax.ShapeDtypeStruct((rows, width), BF16),
@@ -389,27 +499,29 @@
             pltpu.VMEM((model, ff), BF16),
             pltpu.VMEM((ff, model), BF16),
             pltpu.VMEM((tokens, model), BF16),
-            pltpu.VMEM((tokens, TOP_K), jnp.int32),
-            pltpu.VMEM((n_ep, per_expert, model), BF16),
-            pltpu.VMEM((n_ep, per_expert, model), BF16),
-            pltpu.VMEM((n_ep * per_expert, ff), BF16),
-            pltpu.VMEM((n_tp, block_slots, model), BF16),
-            pltpu.VMEM((n_tp, block_slots, model), BF16),
+            pltpu.VMEM((tokens, SUB), F32),
+            pltpu.VMEM((heads, SUB, rows // SUB), F32),
             pltpu.VMEM((n_ep, capacity, model), BF16),
             pltpu.VMEM((n_ep, capacity, model), BF16),
             pltpu.VMEM((block_slots, model), F32),
-            dma((6,)), dma((2,)), dma((2,)), dma((n_ep,)), dma((n_ep,)), dma((n_ep,)), dma((n_ep,)),
-            dma((n_tp,)), dma((n_tp,)), dma((n_ep,)), dma((n_ep,)),
+            rows_of_tp,
+            pltpu.VMEM((n_tp * block_slots, ff), BF16),
+            rows_of_y, rows_of_y, rows_of_y, rows_of_y,
+            pltpu.VMEM((n_ep, capacity, model), BF16),
+            pltpu.VMEM((n_ep, capacity, model), BF16),
+            dma((6,)), dma((2,)), dma((2,)), over_ep, over_ep, over_y, over_y, over_y, over_y,
+            over_y, over_y, over_y, over_y, dma((n_ep,)), dma((n_ep,)), over_ep, over_ep,
         ],
         compiler_params=pltpu.CompilerParams(
             collective_id=0, has_side_effects=True, vmem_limit_bytes=62 * 1024 * 1024
         ),
         name="layer",
     )(
-        x_path, gate_path, conv_taps, decay_gate_w, input_gate_w, decay_rate, decay_shift,
-        expert_in, norm_gain.reshape(1, model), routes, route_scores,
+        x_path, gate_path, conv_taps, decay_gate_w, input_gate_w, decay_rate, decay_shift.T,
+        expert_in, norm_gain.reshape(1, model), routes.T, route_scores.T,
         gate_weight, up_weight, down_weight,
     )
+    return hand_over(recurrent, expert)
 
 
 def solution(mesh):

time: 65.1 us -> 46 us (0.71)
  Pallas kernels: 55.9 us -> 44.7 us
  local copies, waits for them, and re-layouts: 8.23 us -> 0 us
    pallas_call x1, Pallas kernels: 55.9 us -> 42.7 us  [local(): pl.pallas_call(functools.partial(kernel, n_ep, n_tp, capacity), out_shape...]
    unnamed x5 -> x0, local copies, waits for them, and re-layouts: 8.23 us -> none
    pallas_call x0 -> x1, Pallas kernels: none -> 2.07 us  [hand_over(): pl.pallas_call(hand_over_kernel, out_shape=tuple(shapes), in_specs=[hbm,...]
where the time goes in v1:
time: 46 us; the launch traced here: 45.4 us
  Pallas kernels  44.7 us (97%)
  between operations  0.64 us (1%)
    pallas_call x1, Pallas kernels, local(): pl.pallas_call(functools.partial(kernel, n_ep, n_tp, capacity), out_shape...  42.7 us
    pallas_call x1, Pallas kernels, hand_over(): pl.pallas_call(hand_over_kernel, out_shape=tuple(shapes), in_specs=[hbm,...  2.07 us

profile of v1, /device:TPU:1, one launch (start us, length us, event | category | flops | bytes accessed | tf_op | source)
XLA Modules:
  0.0 45.4 jit_solution(5247099948442153652)
XLA Ops:
  0.6 42.7 %layer.1 = (bf16[1024,512]{1,0:T(8,128)(2,1)}, bf16[16,2048]{1,0:T(8,128)(2,1)}) custom-call(bf16[1024,512]{1,0:T(8,128)(2,1)} %x_ref.1, bf16[1024,512]{1,0:T(8,128)(2,1)} %gate_hbm.1, f32[4,512]{1,0:T(4,128)} %taps_ref.1, bf16[2,4,128,128]{3,2,1,0:T(8,128)(2,1)} %dgw_ref.1, bf16[2,4,128,128]{3,2,1,0:T(8,128)(2,1)} %igw_ref.1, f32[2,512]{1,0:T(2,128)} %rate_ref.1, ...), custom_call_target="tpu_custom_call" | custom-call | tf_op jit(solution)/shard_map/layer/pallas_call | solution.py:481
  43.3 2.1 %hand_over.1 = (bf16[1024,512]{1,0:T(8,128)(2,1)}, bf16[16,2048]{1,0:T(8,128)(2,1)}) custom-call(bf16[1024,512]{1,0:T(8,128)(2,1)} %get-tuple-element.4.rec_ref, bf16[16,2048]{1,0:T(8,128)(2,1)} %get-tuple-element.5.exp_ref), custom_call_target="tpu_custom_call" | custom-call | tf_op jit(solution)/shard_map/hand_over/pallas_call | solution.py:450
